TPU v7x, 32 devices: a whole 2x2x4 slice. The times are simulated.
32 devices in a mesh: sp: 8 (over z, y), tp: 4 (over x, core).
Axes of the slice: x: 2, y: 2, z: 4, core: 2. Of those that a mesh axis runs over, the one named last changes fastest.
Arguments:
- moe_input: bfloat16 [2048, 2048], P('sp'), may hold values from -17.5 to 17.5
- cotangent: bfloat16 [2048, 2048], P('sp'), may hold values from -6 to 6
- routes: int32 [2048, 2], P('sp'), may hold values from 0 to 7, all different within a row; in each aligned block of 256 rows (0 to 255, 256 to 511, ...) at most 80 rows name the same one
- route_weights: float32 [2048, 2], P('sp'), may hold values from 0.2 to 1
- gate_weight: bfloat16 [8, 2048, 2048], P('sp', None, 'tp'), may hold values from -0.125 to 0.125
- up_weight: bfloat16 [8, 2048, 2048], P('sp', None, 'tp'), may hold values from -0.125 to 0.125
- down_weight: bfloat16 [8, 2048, 2048], P('sp', 'tp'), may hold values from -0.125 to 0.125
- out_weight: bfloat16 [2048, 2048], P(None, 'tp'), may hold values from -0.125 to 0.125
- mixer_output: bfloat16 [2048, 2048], P('sp', 'tp'), may hold values from -6 to 6
- queries: bfloat16 [2048, 2048], P('sp', 'tp'), may hold values from -6 to 6
- key_vectors: bfloat16 [2048, 2048], P('sp', 'tp'), may hold values from -0.75 to 0.75
- value_vectors: bfloat16 [2048, 2048], P('sp', 'tp'), may hold values from -6 to 6
- log_decay: float32 [2048, 32], P('sp', 'tp'), may hold values from -0.85 to 0
- block_states: bfloat16 [16, 32, 64, 64], P('sp', 'tp'), may hold values from -1.5 to 1.5
Outputs:
- grad_gate: float32 [8, 2048, 2048], P('sp', None, 'tp')
- grad_up: float32 [8, 2048, 2048], P('sp', None, 'tp')
- grad_down: float32 [8, 2048, 2048], P('sp', 'tp')
- grad_out: float32 [2048, 2048], P('sp', 'tp')
- grad_queries: bfloat16 [2048, 2048], P('sp', 'tp')
- grad_keys: bfloat16 [2048, 2048], P('sp', 'tp')
- grad_values: bfloat16 [2048, 2048], P('sp', 'tp')
Inputs may be any that keep to these rules, and one draw needn't show every extreme that they name: `routes`: each row names 2 different experts. Among the rows of one device no expert is named by more than 80 rows, and in every draw some device's rows name some expert exactly 80 times.
All inputs are finite; a program needn't handle non-finite values.
Results may differ from a plain program's by a relative error of at most 0.02.
Values may be sent and summed in bfloat16 or wider, within the bound.
A program may use at most 128 MiB of HBM per device.

v0:
```python
import jax
import jax.numpy as jnp
from jax import lax
from jax.sharding import PartitionSpec as P

EXP_DEV = 1
TOP_K = 2


clamp_limit = 7.0
sigmoid_sharpness = 1.702


def prefix(x, axis, combine, identity):
    peers, place = (lax.axis_size(axis), lax.axis_index(axis))
    everything = jax.tree.map(
        lambda part, kind: lax.all_gather(part.astype(kind), axis), x, (jnp.bfloat16, jnp.bfloat16)
    )
    start = jax.tree.map(
        lambda part, zero: jnp.broadcast_to(jnp.asarray(zero, part.dtype), part.shape), x, identity
    )

    def step(k, before):
        at = peers - 1 - k
        reached = at > place
        new = combine(
            before, jax.tree.map(lambda part, own: part[at].astype(own.dtype), everything, x)
        )
        return jax.tree.map(lambda a, b: jnp.where(reached, a, b), new, before)

    return lax.fori_loop(0, peers, step, start)


def pair_slots(routes, experts_total, capacity):
    flat_routes = routes.reshape(-1)
    onehot = (flat_routes[:, None] == jnp.arange(experts_total, dtype=jnp.int32)[None, :]).astype(
        jnp.int32
    )
    before = jnp.cumsum(onehot, axis=0) - onehot
    return flat_routes * capacity + jnp.sum(before * onehot, axis=1)


def contract_rows(left, right):
    return lax.dot_general(
        left, right, (((0,), (0,)), ((), ())), preferred_element_type=jnp.float32
    )


def contract_cols(left, right):
    return lax.dot_general(
        left, right, (((1,), (1,)), ((), ())), preferred_element_type=jnp.float32
    )


def expert_terms(expert_rows, expert_cotangent, w_gate, w_up, w_down):
    gate_pre = jnp.dot(expert_rows, w_gate, preferred_element_type=jnp.float32)
    up_pre = jnp.dot(expert_rows, w_up, preferred_element_type=jnp.float32)
    act_grad = contract_cols(expert_cotangent, w_down)
    clamped = jnp.minimum(gate_pre, clamp_limit)
    logistic = jax.nn.sigmoid(sigmoid_sharpness * clamped)
    linear = jnp.clip(up_pre, -clamp_limit, clamp_limit)
    activation = (clamped * logistic * (linear + 1.0)).astype(jnp.bfloat16)
    slope_term = logistic + sigmoid_sharpness * clamped * logistic * (1.0 - logistic)
    gate_grad = jnp.where(
        gate_pre < clamp_limit, act_grad * (linear + 1.0) * slope_term, 0.0
    ).astype(jnp.bfloat16)
    up_grad = jnp.where(jnp.abs(up_pre) < clamp_limit, act_grad * clamped * logistic, 0.0).astype(
        jnp.bfloat16
    )
    input_part = contract_cols(gate_grad, w_gate) + contract_cols(up_grad, w_up)
    return (
        input_part,
        contract_rows(expert_rows, gate_grad),
        contract_rows(expert_rows, up_grad),
        contract_rows(activation, expert_cotangent),
    )


def combine_suffix(earlier, later):
    return (earlier[0] * later[0], later[0][:, None, None] * earlier[1] + later[1])


def retention_grads(queries, key_vectors, value_vectors, grad_mix, log_decay, block_states):
    tok_dev = queries.shape[0]
    heads_local = log_decay.shape[1]
    head_dim = queries.shape[1] // heads_local
    blocks = block_states.shape[0]
    block_rows = tok_dev // blocks
    block_shape = (blocks, block_rows, heads_local, head_dim)
    query_blocks = queries.reshape(block_shape)
    key_blocks = key_vectors.reshape(block_shape)
    value_blocks = value_vectors.reshape(block_shape)
    grad_blocks = grad_mix.reshape(block_shape)
    cumulative = jnp.cumsum(log_decay.reshape(blocks, block_rows, heads_local), axis=1)
    block_ends = cumulative[:, -1, :]
    to_end = jnp.exp(block_ends[:, None, :] - cumulative)
    from_start = jnp.exp(cumulative)
    per_attention_head = jnp.transpose(cumulative, (0, 2, 1))
    differences = per_attention_head[:, :, :, None] - per_attention_head[:, :, None, :]
    causal = (
        jnp.arange(block_rows, dtype=jnp.int32)[:, None]
        >= jnp.arange(block_rows, dtype=jnp.int32)[None, :]
    )
    decays = jnp.where(causal, jnp.exp(jnp.minimum(differences, 0.0)), 0.0)
    grad_dot = jnp.einsum(
        "nthe,nshe->nhts", grad_blocks, value_blocks, preferred_element_type=jnp.float32
    )
    weighted_grad = (grad_dot * decays).astype(jnp.bfloat16)
    score_dot = jnp.einsum(
        "nthd,nshd->nhts", query_blocks, key_blocks, preferred_element_type=jnp.float32
    )
    weighted_score = (score_dot * decays).astype(jnp.bfloat16)
    scaled_queries = (query_blocks * from_start[..., None]).astype(jnp.bfloat16)
    outer_terms = jnp.einsum(
        "nthd,nthe->nhde", scaled_queries, grad_blocks, preferred_element_type=jnp.float32
    )
    end_factor = jnp.exp(block_ends)
    local_total = jnp.zeros((heads_local, head_dim, head_dim), jnp.float32)
    for block_id in reversed(range(blocks)):
        local_total = end_factor[block_id][:, None, None] * local_total + outer_terms[block_id]
    device_factor = jnp.exp(jnp.sum(block_ends, axis=0))
    identity = (
        jnp.ones((heads_local,), jnp.float32),
        jnp.zeros((heads_local, head_dim, head_dim), jnp.float32),
    )
    suffix = prefix((device_factor, local_total), "sp", combine_suffix, identity)
    query_intra = jnp.einsum(
        "nhts,nshd->nthd", weighted_grad, key_blocks, preferred_element_type=jnp.float32
    )
    query_carry = jnp.einsum(
        "nthe,nhde->nthd", grad_blocks, block_states, preferred_element_type=jnp.float32
    )
    grad_queries = (
        (query_intra + query_carry * from_start[..., None])
        .astype(jnp.bfloat16)
        .reshape(tok_dev, -1)
    )
    key_intra = jnp.einsum(
        "nhts,nthd->nshd", weighted_grad, query_blocks, preferred_element_type=jnp.float32
    )
    value_intra = jnp.einsum(
        "nhts,nthe->nshe", weighted_score, grad_blocks, preferred_element_type=jnp.float32
    )
    state_grad = suffix[1]
    leaving = []
    for block_id in reversed(range(blocks)):
        leaving.append(state_grad)
        state_grad = end_factor[block_id][:, None, None] * state_grad + outer_terms[block_id]
    carried = jnp.stack(leaving[::-1], axis=0).astype(jnp.bfloat16)
    key_carry = jnp.einsum(
        "nshe,nhde->nshd", value_blocks, carried, preferred_element_type=jnp.float32
    )
    value_carry = jnp.einsum(
        "nshd,nhde->nshe", key_blocks, carried, preferred_element_type=jnp.float32
    )
    grad_keys = (
        (key_intra + key_carry * to_end[..., None]).astype(jnp.bfloat16).reshape(tok_dev, -1)
    )
    grad_values = (
        (value_intra + value_carry * to_end[..., None]).astype(jnp.bfloat16).reshape(tok_dev, -1)
    )
    return (grad_queries, grad_keys, grad_values)


def shards(
    moe_input,
    cotangent,
    routes,
    route_weights,
    gate_weight,
    up_weight,
    down_weight,
    out_weight,
    mixer_output,
    queries,
    key_vectors,
    value_vectors,
    log_decay,
    block_states,
):
    tok_dev, model_width = cotangent.shape
    group_list = lax.axis_size("sp")
    experts_total = EXP_DEV * group_list
    capacity = 5 * tok_dev * TOP_K // (4 * experts_total)
    pair_count = tok_dev * TOP_K
    slot_index = pair_slots(routes, experts_total, capacity)
    slot_pair = (
        jnp.full((experts_total * capacity,), pair_count, jnp.int32)
        .at[slot_index]
        .set(jnp.arange(pair_count, dtype=jnp.int32))
    )
    zero_row = jnp.zeros((1, model_width), jnp.bfloat16)
    scaled = (
        (route_weights[:, :, None] * cotangent[:, None, :])
        .astype(jnp.bfloat16)
        .reshape(pair_count, model_width)
    )
    outgoing_gradients = jnp.concatenate([scaled, zero_row], axis=0)[slot_pair]
    send_inputs = jnp.concatenate([moe_input, zero_row], axis=0)[slot_pair // TOP_K]
    share_width = model_width // lax.axis_size("tp")
    offset = lax.axis_index("tp") * share_width
    part_inputs = lax.dynamic_slice_in_dim(send_inputs, offset, share_width, 1)
    part_grads = lax.dynamic_slice_in_dim(outgoing_gradients, offset, share_width, 1)
    arrived_parts = (
        lax.all_to_all(part_inputs, "sp", split_axis=0, concat_axis=0, tiled=True),
        lax.all_to_all(part_grads, "sp", split_axis=0, concat_axis=0, tiled=True),
    )
    arrived_inputs, arrived_grads = (
        lax.all_gather(arrived_parts[0], "tp", axis=1, tiled=True),
        lax.all_gather(arrived_parts[1], "tp", axis=1, tiled=True),
    )
    arrived_inputs = arrived_inputs.reshape(group_list, EXP_DEV, capacity, model_width)
    arrived_grads = arrived_grads.reshape(group_list, EXP_DEV, capacity, model_width)
    outcomes = [
        expert_terms(
            arrived_inputs[:, 0].reshape(group_list * capacity, model_width),
            arrived_grads[:, 0].reshape(group_list * capacity, model_width),
            gate_weight[0],
            up_weight[0],
            down_weight[0],
        )
    ]
    input_part = jnp.stack(
        [outcome[0].reshape(group_list, capacity, model_width) for outcome in outcomes], axis=1
    )
    input_part = input_part.reshape(group_list * EXP_DEV * capacity, model_width)
    grad_gate = jnp.stack([outcome[1] for outcome in outcomes], axis=0)
    grad_up = jnp.stack([outcome[2] for outcome in outcomes], axis=0)
    grad_down = jnp.stack([outcome[3] for outcome in outcomes], axis=0)
    shares = lax.psum_scatter(
        input_part.astype(jnp.bfloat16), "tp", scatter_dimension=1, tiled=True
    )
    returned_part = lax.all_to_all(shares, "sp", split_axis=0, concat_axis=0, tiled=True)
    returned = lax.all_gather(returned_part, "tp", axis=1, tiled=True)
    pair_grads = returned[slot_index].reshape(tok_dev, TOP_K, model_width).astype(jnp.float32)
    residual_grad = (cotangent.astype(jnp.float32) + jnp.sum(pair_grads, axis=1)).astype(
        jnp.bfloat16
    )
    grad_out = lax.psum_scatter(
        contract_rows(residual_grad, mixer_output).astype(jnp.bfloat16),
        "sp",
        scatter_dimension=0,
        tiled=True,
    ).astype(jnp.float32)
    grad_mix = jnp.dot(residual_grad, out_weight, preferred_element_type=jnp.float32).astype(
        jnp.bfloat16
    )
    grad_queries, grad_keys, grad_values = retention_grads(
        queries, key_vectors, value_vectors, grad_mix, log_decay, block_states
    )
    return (grad_gate, grad_up, grad_down, grad_out, grad_queries, grad_keys, grad_values)


def solution(mesh):
    return jax.shard_map(
        shards,
        mesh=mesh,
        in_specs=(
            P("sp", None),
            P("sp", None),
            P("sp", None),
            P("sp", None),
            P("sp", None, "tp"),
            P("sp", None, "tp"),
            P("sp", "tp", None),
            P(None, "tp"),
            P("sp", "tp"),
            P("sp", "tp"),
            P("sp", "tp"),
            P("sp", "tp"),
            P("sp", "tp"),
            P("sp", "tp", None, None),
        ),
        out_specs=(
            P("sp", None, "tp"),
            P("sp", None, "tp"),
            P("sp", "tp", None),
            P("sp", "tp"),
            P("sp", "tp"),
            P("sp", "tp"),
            P("sp", "tp"),
        ),
        check_vma=False,
    )
```

profile of v0, /device:TPU:0, one launch (start us, length us, event | category | flops | bytes accessed | tf_op | source)
XLA Modules:
  0.0 360.6 jit_solution(15607565252938917201)
XLA Ops:
  14.8 4.1 %gather_fusion = bf16[640,2048]{1,0:T(8,128)(2,1)} fusion(bf16[257,2048]{1,0:T(8,128)(2,1)S(1)} %concatenate.6, s32[1024]{0:T(1024)S(1)} %get-tuple-element.195), kind=kCustom, calls=%fused_computation | custom fusion | bytes 5245440 | tf_op jit(solution)/shard_map/gather | solution.py:199
  20.0 24.9 %all_to_all.36 = bf16[8,80,512]{2,1,0:T(8,128)(2,1)} all-to-all(bf16[8,80,512]{2,1,0:T(8,128)(2,1)S(1)} %bitcast.133), channel_id=1, replica_groups=mesh['sp'=8,'tp'=4] {'sp'}, dimensions={0} | all-to-all | bytes 1310720 | tf_op jit(solution)/shard_map/all_to_all | solution.py:205
  45.0 4.2 %mul.168 = f32[256,2,2048]{2,1,0:T(2,128)} broadcast(bf16[256,2048]{1,0:T(8,128)(2,1)S(1)} %copy-done.2), dimensions={0,2} | broadcast | bytes 5242880 | tf_op jit(solution)/shard_map/mul | solution.py:194
  49.2 6.3 %mul.169 = f32[512,2048]{1,0:T(8,128)} reshape(f32[256,2,2048]{2,1,0:T(2,128)} %mul.168) | data formatting | bytes 8388608 | tf_op jit(solution)/shard_map/mul | solution.py:194
  59.8 8.8 %gather_fusion.1 = bf16[640,2048]{1,0:T(8,128)(2,1)} fusion(bf16[513,2048]{1,0:T(8,128)(2,1)} %concatenate.7, s32[1024]{0:T(1024)S(1)} %get-tuple-element.194), kind=kCustom, calls=%fused_computation.1 | custom fusion | bytes 5245440 | tf_op jit(solution)/shard_map/gather | solution.py:198
  69.7 20.5 %all_to_all.37 = bf16[8,80,512]{2,1,0:T(8,128)(2,1)} all-to-all(bf16[8,80,512]{2,1,0:T(8,128)(2,1)S(1)} %bitcast.132), channel_id=1, replica_groups=mesh['sp'=8,'tp'=4] {'sp'}, dimensions={0} | all-to-all | bytes 1310720 | tf_op jit(solution)/shard_map/all_to_all | solution.py:206
  90.5 5.2 %fusion.2 = f32[640,512]{1,0:T(8,128)} fusion(bf16[640,2048]{1,0:T(8,128)(2,1)} %all-gather.5.cloned.1.call-done, bf16[1,2048,512]{2,1,0:T(8,128)(2,1)} %param.21), kind=kOutput, calls=%fused_computation.14 | convolution fusion | flops 1342177280 | bytes 6029312 | tf_op jit(solution)/shard_map/dot_general | solution.py:57
  95.7 2.6 fusion.8
  98.3 16.2 %all-gather.7.cloned.1.call-done = bf16[640,2048]{1,0:T(8,128)(2,1)} async-done(((bf16[640,512]{1,0:T(8,128)(2,1)}), bf16[640,2048]{1,0:T(8,128)(2,1)}) %all-gather.7.cloned.1.call-update) | async-done | bytes 2621456 | tf_op jit(solution)/shard_map/all_gather | solution.py:210
  114.6 5.4 %select_convert_fusion = (bf16[640,512]{1,0:T(8,128)(2,1)S(1)}, bf16[640,512]{1,0:T(8,128)(2,1)S(1)}) fusion(f32[640,512]{1,0:T(8,128)} %fusion.2, f32[640,512]{1,0:T(8,128)} %fusion.8, bf16[640,2048]{1,0:T(8,128)(2,1)} %all-gather.7.cloned.1.call-done, bf16[1,512,2048]{2,1,0:T(8,128)(2,1)} %param.22), kind=kOutput, calls=%fused_computation.26 | convolution fusion | flops 1349386240 | bytes 8650752 | tf_op jit(solution)/shard_map/dot_general | solution.py:50
  122.1 3.1 add_convert_fusion
  125.2 34.4 %reduce-scatter.3.cloned.1.call-done = bf16[640,512]{1,0:T(8,128)(2,1)} async-done(((bf16[640,2048]{1,0:T(8,128)(2,1)}), bf16[640,512]{1,0:T(8,128)(2,1)}) %reduce-scatter.3.cloned.1.call-update) | async-done | bytes 655376 | tf_op jit(solution)/shard_map/reduce_scatter | solution.py:230
  159.7 23.3 %all_to_all.38 = bf16[8,80,512]{2,1,0:T(8,128)(2,1)} all-to-all(bf16[8,80,512]{2,1,0:T(8,128)(2,1)} %bitcast.135), channel_id=1, replica_groups=mesh['sp'=8,'tp'=4] {'sp'}, dimensions={0} | all-to-all | bytes 1310720 | tf_op jit(solution)/shard_map/all_to_all | solution.py:233
  186.4 19.3 %all-reduce.2 = bf16[64]{0:T(256)(128)(2,1)S(1)} all-reduce(bf16[64]{0:T(256)(128)(2,1)S(1)} %dynamic-update-slice), channel_id=2, replica_groups=mesh['sp'=8,'tp'=4] {'sp'}, use_global_device_ids=true, to_apply=%add.2 | all-reduce | flops 64 | bytes 256
  208.6 5.7 %convolution_bitcast_fusion.1 = f32[1,2048,512]{2,1,0:T(8,128)} fusion(bf16[640,2048]{1,0:T(8,128)(2,1)} %all-gather.5.cloned.1.call-done, bf16[640,512]{1,0:T(8,128)(2,1)S(1)} %copy-done.13), kind=kOutput, calls=%fused_computation.10 | convolution fusion | flops 1342177280 | bytes 7471104 | tf_op jit(solution)/shard_map/dot_general | solution.py:44
  214.4 3.9 %convolution_bitcast_fusion.2 = f32[1,2048,512]{2,1,0:T(8,128)} fusion(bf16[640,2048]{1,0:T(8,128)(2,1)S(1)} %copy-done.22, bf16[640,512]{1,0:T(8,128)(2,1)S(1)} %copy-done.11), kind=kOutput, calls=%fused_computation.11 | convolution fusion | flops 1342177280 | bytes 7471104 | tf_op jit(solution)/shard_map/dot_general | solution.py:44
  218.3 4.0 %convolution_bitcast_fusion = f32[1,512,2048]{2,1,0:T(8,128)} fusion(bf16[640,2048]{1,0:T(8,128)(2,1)S(1)} %copy-done.23, f32[640,512]{1,0:T(8,128)S(1)} %copy-done.26, f32[640,512]{1,0:T(8,128)S(1)} %copy-done.25), kind=kOutput, calls=%fused_computation.9 | convolution fusion | flops 1345454080 | bytes 9437184 | tf_op jit(solution)/shard_map/dot_general | solution.py:44
  222.3 6.5 %gather_fusion.2 = bf16[512,2048]{1,0:T(8,128)(2,1)S(1)} fusion(bf16[640,2048]{1,0:T(8,128)(2,1)} %all-gather.9.cloned.1.call-done, s32[1024]{0:T(1024)S(1)} %pad_clamp_fusion), kind=kCustom, calls=%fused_computation.2 | custom fusion | bytes 4196352 | tf_op jit(solution)/shard_map/gather | solution.py:235
  228.8 4.2 %reshape.148 = f32[256,2,2048]{2,1,0:T(2,128)} reshape(bf16[512,2048]{1,0:T(8,128)(2,1)S(1)} %gather_fusion.2) | data formatting | bytes 6291456 | tf_op jit(solution)/shard_map/convert_element_type | solution.py:235
  233.0 7.2 %reduce_sum.31 = f32[256,2048]{1,0:T(8,128)S(1)} reduce(f32[256,2,2048]{2,1,0:T(2,128)} %reshape.148, f32[]{:T(128)} %constant.100.clone.1), dimensions={1}, to_apply=%region_5.6 | reduce | flops 524288 | bytes 6291460 | tf_op jit(solution)/shard_map/reduce_sum | solution.py:236
  240.2 3.0 convolution_convert_fusion.1
  249.6 35.2 %all_gather.21 = bf16[8,8,64,64]{3,2,1,0:T(8,128)(2,1)} all-gather(bf16[1,8,64,64]{3,2,1,0:T(8,128)(2,1)S(1)} %fusion.30), channel_id=1, replica_groups=mesh['sp'=8,'tp'=4] {'sp'}, dimensions={0}, use_global_device_ids=true | all-gather | bytes 589824 | tf_op jit(solution)/shard_map/all_gather | solution.py:17
  286.9 8.6 %while.16 = (s32[]{:T(128)}, f32[8,64,64]{2,1,0:T(8,128)S(1)}, s32[]{:T(128)}, bf16[8,8]{1,0:T(8,128)(2,1)S(1)}, bf16[8,8,64,64]{3,2,1,0:T(8,128)(2,1)}, /*index=5*/s32[]{:T(128)}, s32[]{:T(128)}, s32[]{:T(128)}, s32[]{:T(128)}) while((s32[]{:T(128)}, f32[8,64,64]{2,1,0:T(8,128)S(1)}, s32[]{:T(128)}, ...), condition=%wide.region_10.11_spmd.clone, body=%wide.region_9.10_spmd.clone.sunk | while | flops 163856 | bytes 327927 | solution.py:31
  302.4 49.4 %reduce-scatter.5.cloned.1.call-done = bf16[256,512]{1,0:T(8,128)(2,1)} async-done(((bf16[2048,512]{1,0:T(8,128)(2,1)}), bf16[256,512]{1,0:T(8,128)(2,1)}) %reduce-scatter.5.cloned.1.call-update) | async-done | bytes 262160 | tf_op jit(solution)/shard_map/reduce_scatter | solution.py:239
  (151 shorter events, 47.4 us)
Async XLA Ops:
  7.2 88.6 %copy-start = (bf16[1,2048,512]{2,1,0:T(8,128)(2,1)S(1)}, bf16[1,2048,512]{2,1,0:T(8,128)(2,1)}, u32[]{:S(2)}) copy-start(bf16[1,2048,512]{2,1,0:T(8,128)(2,1)} %param.20) | copy-start | bytes 6291460
  7.2 83.3 %all-gather.5.cloned.1.call-start = ((), (), s32[]{:S(2)}) async-start(), calls=%async_computation.5 | async-start | bytes 3276800 | tf_op jit(solution)/shard_map/all_gather | solution.py:209
  18.8 26.2 %copy-start.2 = (bf16[256,2048]{1,0:T(8,128)(2,1)S(1)}, bf16[256,2048]{1,0:T(8,128)(2,1)}, u32[]{:S(2)}) copy-start(bf16[256,2048]{1,0:T(8,128)(2,1)} %param.17) | copy-start | bytes 3145732
  45.0 69.6 %all-gather.7.cloned.1.call-start = ((), (), s32[]{:S(2)}) async-start(), calls=%async_computation.6 | async-start | bytes 3276800 | tf_op jit(solution)/shard_map/all_gather | solution.py:210
  49.2 6.3 %copy-start.20 = (f32[256,2]{0,1:T(2,128)S(1)}, f32[256,2]{0,1:T(2,128)}, u32[]{:S(2)}) copy-start(f32[256,2]{0,1:T(2,128)} %param.19) | copy-start | bytes 6148
  90.3 69.4 %reduce-scatter.3.cloned.1.call-start = ((), (), s32[]{:S(2)}) async-start(), calls=%async_computation.7 | async-start | bytes 3276800 | tf_op jit(solution)/shard_map/reduce_scatter | solution.py:230
  90.5 5.2 %copy-start.21 = (bf16[640,2048]{1,0:T(8,128)(2,1)S(1)}, bf16[640,2048]{1,0:T(8,128)(2,1)}, u32[]{:S(2)}) copy-start(bf16[640,2048]{1,0:T(8,128)(2,1)} %all-gather.5.cloned.1.call-done) | copy-start | bytes 7864324
  125.1 57.9 %copy-start.19 = (f32[256,8]{0,1:T(8,128)S(1)}, f32[256,8]{0,1:T(8,128)}, u32[]{:S(2)}) copy-start(f32[256,8]{0,1:T(8,128)} %param.28) | copy-start | bytes 24580
  125.1 58.4 %copy-start.14 = (bf16[256,512]{1,0:T(8,128)(2,1)S(1)}, bf16[256,512]{1,0:T(8,128)(2,1)}, u32[]{:S(2)}) copy-start(bf16[256,512]{1,0:T(8,128)(2,1)} %param.25) | copy-start | bytes 786436
  125.2 97.1 %all-gather.9.cloned.1.call-start = ((), (), s32[]{:S(2)}) async-start(), calls=%async_computation.8 | async-start | bytes 3276800 | tf_op jit(solution)/shard_map/all_gather | solution.py:234
  159.7 25.2 %copy-start.24 = (u32[32]{0:T(128)S(1)}, u32[32]{0:T(128)}, u32[]{:S(2)}) copy-start(u32[32]{0:T(128)} %constant.113) | copy-start | bytes 388
  159.7 46.2 %copy-start.15 = (bf16[256,512]{1,0:T(8,128)(2,1)S(1)}, bf16[256,512]{1,0:T(8,128)(2,1)}, u32[]{:S(2)}) copy-start(bf16[256,512]{1,0:T(8,128)(2,1)} %param.26) | copy-start | bytes 786436
  183.0 168.9 %reduce-scatter.5.cloned.1.call-start = ((), (), s32[]{:S(2)}) async-start(), calls=%async_computation.9 | async-start | bytes 2359296 | tf_op jit(solution)/shard_map/reduce_scatter | solution.py:239
  183.2 24.0 %copy-start.16 = (bf16[256,512]{1,0:T(8,128)(2,1)S(1)}, bf16[256,512]{1,0:T(8,128)(2,1)}, u32[]{:S(2)}) copy-start(bf16[256,512]{1,0:T(8,128)(2,1)} %param.27) | copy-start | bytes 786436
  183.8 24.8 %copy-start.13 = (bf16[640,512]{1,0:T(8,128)(2,1)S(1)}, bf16[640,512]{1,0:T(8,128)(2,1)}, u32[]{:S(2)}) copy-start(bf16[640,512]{1,0:T(8,128)(2,1)} %copy-done.12) | copy-start | bytes 1966084
  208.6 5.8 %copy-start.11 = (bf16[640,512]{1,0:T(8,128)(2,1)S(1)}, bf16[640,512]{1,0:T(8,128)(2,1)}, u32[]{:S(2)}) copy-start(bf16[640,512]{1,0:T(8,128)(2,1)} %copy-done.10) | copy-start | bytes 1966084
  208.6 5.8 %copy-start.22 = (bf16[640,2048]{1,0:T(8,128)(2,1)S(1)}, bf16[640,2048]{1,0:T(8,128)(2,1)}, u32[]{:S(2)}) copy-start(bf16[640,2048]{1,0:T(8,128)(2,1)} %all-gather.5.cloned.1.call-done) | copy-start | bytes 7864324
  214.4 3.9 %copy-start.25 = (f32[640,512]{1,0:T(8,128)S(1)}, f32[640,512]{1,0:T(8,128)}, u32[]{:S(2)}) copy-start(f32[640,512]{1,0:T(8,128)} %fusion.2) | copy-start | bytes 3932164
  247.3 37.4 %copy-start.18 = (bf16[256,512]{1,0:T(8,128)(2,1)S(1)}, bf16[256,512]{1,0:T(8,128)(2,1)}, u32[]{:S(2)}) copy-start(bf16[256,512]{1,0:T(8,128)(2,1)} %param.24) | copy-start | bytes 786436
  286.9 8.7 %copy-start.4 = (f32[2,8,64,64]{3,2,1,0:T(8,128)S(1)}, f32[2,8,64,64]{3,2,1,0:T(8,128)}, u32[]{:S(2)}) copy-start(f32[2,8,64,64]{3,2,1,0:T(8,128)} %copy-done.3) | copy-start | bytes 786436
  286.9 8.8 %copy-start.5 = (bf16[2,128,8,64]{1,3,2,0:T(8,128)(2,1)S(1)}, bf16[2,128,8,64]{1,3,2,0:T(8,128)(2,1)}, u32[]{:S(2)}) copy-start(bf16[2,128,8,64]{1,3,2,0:T(8,128)(2,1)} %copy.77) | copy-start | bytes 786436
  286.9 8.8 %copy-start.6 = (bf16[2,128,8,64]{1,3,2,0:T(8,128)(2,1)S(1)}, bf16[2,128,8,64]{1,3,2,0:T(8,128)(2,1)}, u32[]{:S(2)}) copy-start(bf16[2,128,8,64]{1,3,2,0:T(8,128)(2,1)} %copy.82) | copy-start | bytes 786436
  286.9 8.8 %copy-start.7 = (bf16[2,128,8,64]{1,3,2,0:T(8,128)(2,1)S(1)}, bf16[2,128,8,64]{1,3,2,0:T(8,128)(2,1)}, u32[]{:S(2)}) copy-start(bf16[2,128,8,64]{1,3,2,0:T(8,128)(2,1)} %copy.71) | copy-start | bytes 786436
  300.4 53.2 %copy-start.1 = (bf16[1,2048,512]{2,1,0:T(8,128)(2,1)S(1)}, bf16[1,2048,512]{2,1,0:T(8,128)(2,1)}, u32[]{:S(2)}) copy-start(bf16[1,2048,512]{2,1,0:T(8,128)(2,1)} %param.20) | copy-start | bytes 6291460
  (8 other events, 18.1 us)
Sparse Core Ops, SparseCore 0:
  45.1 24.1 all-gather.4
  90.4 24.1 all-gather.6
  125.3 34.3 reduce-scatter.2
  183.1 23.2 all-gather.8
  287.0 64.7 reduce-scatter.4
where the time goes:
time: 368 us; the launch traced here: 361 us
  blocking collectives  123 us (33%)
  waiting for transfers between devices  100 us (27%)
  local copies, waits for them, and re-layouts  58.3 us (16%)
  matrix products  40.6 us (11%)
  other arithmetic  22.3 us (6%)
  between operations  15.4 us (4%)
    reduce_scatter x1, waiting for transfers between devices, shards(): lax.psum_scatter(contract_rows(residual_grad, mixer_output).astype(jnp.bf...  49.4 us
    all_gather x1, blocking collectives, prefix(): lax.all_gather(part.astype(kind), axis)  35.2 us
    reduce_scatter x1, waiting for transfers between devices, shards(): lax.psum_scatter(input_part.astype(jnp.bfloat16), 'tp', scatter_dimension...  34.4 us
    all_to_all x1, blocking collectives, shards(): lax.all_to_all(part_inputs, 'sp', split_axis=0, concat_axis=0, tiled=True)  24.9 us
    all_to_all x1, blocking collectives, shards(): lax.all_to_all(shares, 'sp', split_axis=0, concat_axis=0, tiled=True)  23.3 us
    all_to_all x1, blocking collectives, shards(): lax.all_to_all(part_grads, 'sp', split_axis=0, concat_axis=0, tiled=True)  20.5 us
    unnamed x1, blocking collectives  19.3 us
    all_gather x1, waiting for transfers between devices, shards(): lax.all_gather(arrived_parts[1], 'tp', axis=1, tiled=True)  16.2 us
  transfers between devices with their start and end apart: 5, of which 3 were waited for; matrix products, arithmetic and copies ran while one was open for 18% of the time, Pallas kernels for 0%

commit v1 on v0

v1 whole, which is shorter than its diff:
```python
import functools

import jax
import jax.numpy as jnp
from jax import lax
from jax.experimental import pallas as pl
from jax.experimental.pallas import tpu as pltpu
from jax.sharding import PartitionSpec as P

TOP_K = 2
MESH = pl.DeviceIdType.MESH
VMEM = pl.BlockSpec(memory_space=pltpu.VMEM)
ANY = pl.BlockSpec(memory_space=pl.ANY)

clamp_limit = 7.0
sigmoid_sharpness = 1.702


def contract_rows(left, right):
    return lax.dot_general(
        left, right, (((0,), (0,)), ((), ())), preferred_element_type=jnp.float32
    )


def contract_cols(left, right):
    return lax.dot_general(
        left, right, (((1,), (1,)), ((), ())), preferred_element_type=jnp.float32
    )


def peer_order(peers):
    near = [k for k in range(1, peers) if k < peers // 2]
    far = [k for k in range(1, peers) if k >= peers // 2]
    order = []
    while near or far:
        if near:
            order.append(near.pop(0))
        if far:
            order.append(far.pop(0))
    return order


def greet(peers, sp, tp):
    barrier = pltpu.get_barrier_semaphore()
    others = [(sp ^ k, tp) for k in range(1, peers)] + [(sp, tp ^ 1), (sp, tp ^ 2)]
    for other in others:
        pl.semaphore_signal(barrier, inc=1, device_id=other, device_id_type=MESH)
    pl.semaphore_wait(barrier, len(others))


def remote(src, dst, sems, kind, at, device):
    return pltpu.make_async_remote_copy(
        src_ref=src,
        dst_ref=dst,
        send_sem=sems.at[(2 * kind,) + at],
        recv_sem=sems.at[(2 * kind + 1,) + at],
        device_id=device,
        device_id_type=MESH,
    )


def exchange_start(peers, sp, tp, arrays, source, chunk, sems, local_sems):
    order = peer_order(peers)
    owns, firsts = [], {}
    for k in order:
        for a, (src, dst) in enumerate(arrays):
            copy = remote(source(src, sp ^ k), chunk(dst, sp, tp), sems, 0, (a, k), (sp ^ k, tp))
            copy.start()
            firsts[a, k] = copy
    for a, (src, dst) in enumerate(arrays):
        copy = pltpu.make_async_copy(source(src, sp), chunk(dst, sp, tp), local_sems.at[a])
        copy.start()
        owns.append(copy)
    return order, owns, firsts


def exchange_finish(peers, sp, tp, arrays, source, chunk, sems, state):
    order, owns, firsts = state
    crossings, partners, forwards = {}, {}, {}

    def forward(k):
        for a, (_, dst) in enumerate(arrays):
            crossings[a, k].wait_recv()
            here = chunk(dst, sp ^ k, tp ^ 2)
            copy = remote(here, here, sems, 3, (a, k), (sp, tp ^ 1))
            copy.start()
            forwards[a, k] = copy

    steps = [0] + order
    for i, k in enumerate(steps):
        for a, (src, dst) in enumerate(arrays):
            there = chunk(dst, sp ^ k, tp)
            if k:
                firsts[a, k].wait_recv()
                here = there
            else:
                here = source(src, sp)
            copy = remote(here, there, sems, 1, (a, k), (sp, tp ^ 2))
            copy.start()
            crossings[a, k] = copy
            copy = remote(here, there, sems, 2, (a, k), (sp, tp ^ 1))
            copy.start()
            partners[a, k] = copy
        if i >= 1:
            forward(steps[i - 1])
    forward(steps[-1])
    for copy in owns:
        copy.wait()
    for group in (partners, forwards):
        for copy in group.values():
            copy.wait_recv()
    for group in (firsts, crossings, partners, forwards):
        for copy in group.values():
            copy.wait_send()


def dispatch_kernel(peers, x_ref, g_ref, ox_ref, og_ref, sems, local_sems):
    sp, tp = lax.axis_index("sp"), lax.axis_index("tp")
    width = x_ref.shape[2]
    greet(peers, sp, tp)

    def source(ref, s):
        return ref.at[s]

    def chunk(ref, s, t):
        return ref.at[s, :, pl.ds(pl.multiple_of(t * width, width), width)]

    arrays = ((x_ref, ox_ref), (g_ref, og_ref))
    state = exchange_start(peers, sp, tp, arrays, source, chunk, sems, local_sems)
    exchange_finish(peers, sp, tp, arrays, source, chunk, sems, state)


def dispatch(x, g, parts):
    peers, capacity, width = x.shape
    out = jax.ShapeDtypeStruct((peers, capacity, width * parts), jnp.bfloat16)
    return pl.pallas_call(
        functools.partial(dispatch_kernel, peers),
        out_shape=(out, out),
        in_specs=[ANY, ANY],
        out_specs=(ANY, ANY),
        scratch_shapes=[
            pltpu.SemaphoreType.DMA((8, 2, peers)),
            pltpu.SemaphoreType.DMA((2,)),
        ],
        compiler_params=pltpu.CompilerParams(collective_id=0, has_side_effects=True),
        name="dispatch",
    )(x, g)


def return_kernel(
    peers, part_ref, pick_ref, cot_ref, res_ref, rx1, acc, sb, rx2, fb, ret, sems, tail_sems
):
    sp, tp = lax.axis_index("sp"), lax.axis_index("tp")
    width = cot_ref.shape[1]
    greet(peers, sp, tp)
    steps = peer_order(peers)[::-1] + [0]

    def cols(t):
        return pl.ds(pl.multiple_of(t * width, width), width)

    firsts, crossings, homes = {}, {}, {}
    for k in steps:
        for half, t in ((0, tp ^ 1), (1, tp ^ 3)):
            copy = remote(
                part_ref.at[sp ^ k, :, cols(t)], rx1.at[half, k], sems, half, (k,), (sp, tp ^ 1)
            )
            copy.start()
            firsts[half, k] = copy

    def cross(k):
        firsts[1, k].wait_recv()
        sb[k] = (
            part_ref[sp ^ k, :, cols(tp ^ 2)].astype(jnp.float32)
            + rx1[1, k].astype(jnp.float32)
        ).astype(jnp.bfloat16)
        crossings[k] = remote(sb.at[k], rx2.at[k], sems, 2, (k,), (sp, tp ^ 2))
        crossings[k].start()
        firsts[0, k].wait_recv()
        acc[k] = part_ref[sp ^ k, :, cols(tp)].astype(jnp.float32) + rx1[0, k].astype(
            jnp.float32
        )

    def home(k):
        crossings[k].wait_recv()
        final = (acc[k] + rx2[k].astype(jnp.float32)).astype(jnp.bfloat16)
        if k:
            fb[k] = final
            homes[k] = remote(fb.at[k], ret.at[sp], sems, 3, (k,), (sp ^ k, tp))
            homes[k].start()
        else:
            ret[sp] = final

    for i, k in enumerate(steps):
        cross(k)
        if i >= 2:
            home(steps[i - 2])
    home(steps[-2])
    home(steps[-1])
    total = cot_ref[...].astype(jnp.float32)
    for k in [0] + [k for k in steps if k]:
        if k:
            homes[k].wait_recv()
        total = total + jnp.dot(
            pick_ref[sp ^ k], ret[sp ^ k], preferred_element_type=jnp.float32
        )
    res_ref[:, cols(tp)] = total.astype(jnp.bfloat16)
    mine = res_ref.at[:, cols(tp)]
    across = remote(mine, mine, tail_sems, 0, (), (sp, tp ^ 2))
    across.start()
    beside = remote(mine, mine, tail_sems, 1, (), (sp, tp ^ 1))
    beside.start()
    across.wait_recv()
    theirs = res_ref.at[:, cols(tp ^ 2)]
    onward = remote(theirs, theirs, tail_sems, 2, (), (sp, tp ^ 1))
    onward.start()
    beside.wait_recv()
    onward.wait_recv()
    for group in (firsts, crossings, homes):
        for copy in group.values():
            copy.wait_send()
    for copy in (across, beside, onward):
        copy.wait_send()


def return_rows(part, pick, cot):
    peers, capacity, full = part.shape
    tokens, width = cot.shape
    rows = (peers, capacity, width)
    return pl.pallas_call(
        functools.partial(return_kernel, peers),
        out_shape=jax.ShapeDtypeStruct((tokens, full), jnp.bfloat16),
        in_specs=[VMEM] * 3,
        out_specs=VMEM,
        scratch_shapes=[
            pltpu.VMEM((2,) + rows, jnp.bfloat16),
            pltpu.VMEM(rows, jnp.float32),
            pltpu.VMEM(rows, jnp.bfloat16),
            pltpu.VMEM(rows, jnp.bfloat16),
            pltpu.VMEM(rows, jnp.bfloat16),
            pltpu.VMEM(rows, jnp.bfloat16),
            pltpu.SemaphoreType.DMA((8, peers)),
            pltpu.SemaphoreType.DMA((6,)),
        ],
        compiler_params=pltpu.CompilerParams(
            collective_id=1, has_side_effects=True, vmem_limit_bytes=40 * 2**20
        ),
        name="return_rows",
    )(part, pick, cot)


def final_kernel(
    peers, parts, res_ref, tot_ref, log_ref, all_res, all_tot, all_log, sems, local_sems, st_sems
):
    sp, tp = lax.axis_index("sp"), lax.axis_index("tp")
    share = res_ref.shape[1] // parts
    greet(peers, sp, tp)

    def rows(t):
        return pl.ds(pl.multiple_of(t * share, share), share)

    def source(ref, s):
        return ref.at[s, rows(tp)]

    def chunk(ref, s, t):
        return ref.at[s, rows(t)]

    small = []
    for k in peer_order(peers):
        for i, (src, dst) in enumerate(((tot_ref, all_tot), (log_ref, all_log))):
            copy = remote(src, dst.at[sp], st_sems, i, (k,), (sp ^ k, tp))
            copy.start()
            small.append(copy)
    own = []
    for i, (src, dst) in enumerate(((tot_ref, all_tot), (log_ref, all_log))):
        copy = pltpu.make_async_copy(src, dst.at[sp], local_sems.at[1 + i])
        copy.start()
        own.append(copy)
    arrays = ((res_ref, all_res),)
    state = exchange_start(peers, sp, tp, arrays, source, chunk, sems, local_sems)
    exchange_finish(peers, sp, tp, arrays, source, chunk, sems, state)
    for copy in own + small:
        copy.wait()


def final_exchange(res, tot, logs, parts):
    peers = res.shape[0]
    return pl.pallas_call(
        functools.partial(final_kernel, peers, parts),
        out_shape=(
            jax.ShapeDtypeStruct(res.shape, res.dtype),
            jax.ShapeDtypeStruct((peers,) + tot.shape, tot.dtype),
            jax.ShapeDtypeStruct((peers,) + logs.shape, logs.dtype),
        ),
        in_specs=[ANY] * 3,
        out_specs=(ANY,) * 3,
        scratch_shapes=[
            pltpu.SemaphoreType.DMA((8, 1, peers)),
            pltpu.SemaphoreType.DMA((3,)),
            pltpu.SemaphoreType.DMA((4, peers)),
        ],
        compiler_params=pltpu.CompilerParams(collective_id=2, has_side_effects=True),
        name="final_exchange",
    )(res, tot, logs)


def pair_slots(routes, experts_total, capacity):
    flat_routes = routes.reshape(-1)
    onehot = (flat_routes[:, None] == jnp.arange(experts_total, dtype=jnp.int32)[None, :]).astype(
        jnp.int32
    )
    before = jnp.cumsum(onehot, axis=0) - onehot
    return flat_routes * capacity + jnp.sum(before * onehot, axis=1)


def expert_terms(expert_rows, expert_cotangent, w_gate, w_up, w_down):
    gate_pre = jnp.dot(expert_rows, w_gate, preferred_element_type=jnp.float32)
    up_pre = jnp.dot(expert_rows, w_up, preferred_element_type=jnp.float32)
    act_grad = contract_cols(expert_cotangent, w_down)
    clamped = jnp.minimum(gate_pre, clamp_limit)
    logistic = jax.nn.sigmoid(sigmoid_sharpness * clamped)
    linear = jnp.clip(up_pre, -clamp_limit, clamp_limit)
    activation = (clamped * logistic * (linear + 1.0)).astype(jnp.bfloat16)
    slope_term = logistic + sigmoid_sharpness * clamped * logistic * (1.0 - logistic)
    gate_grad = jnp.where(
        gate_pre < clamp_limit, act_grad * (linear + 1.0) * slope_term, 0.0
    ).astype(jnp.bfloat16)
    up_grad = jnp.where(jnp.abs(up_pre) < clamp_limit, act_grad * clamped * logistic, 0.0).astype(
        jnp.bfloat16
    )
    input_part = contract_cols(gate_grad, w_gate) + contract_cols(up_grad, w_up)
    return (
        input_part,
        contract_rows(expert_rows, gate_grad),
        contract_rows(expert_rows, up_grad),
        contract_rows(activation, expert_cotangent),
    )


def retention_grads(
    queries, key_vectors, value_vectors, grad_mix, log_decay, block_states, exchange
):
    tok_dev = queries.shape[0]
    heads_local = log_decay.shape[1]
    head_dim = queries.shape[1] // heads_local
    blocks = block_states.shape[0]
    block_rows = tok_dev // blocks
    block_shape = (blocks, block_rows, heads_local, head_dim)
    query_blocks = queries.reshape(block_shape)
    key_blocks = key_vectors.reshape(block_shape)
    value_blocks = value_vectors.reshape(block_shape)
    grad_blocks = grad_mix.reshape(block_shape)
    cumulative = jnp.cumsum(log_decay.reshape(blocks, block_rows, heads_local), axis=1)
    block_ends = cumulative[:, -1, :]
    to_end = jnp.exp(block_ends[:, None, :] - cumulative)
    from_start = jnp.exp(cumulative)
    per_attention_head = jnp.transpose(cumulative, (0, 2, 1))
    differences = per_attention_head[:, :, :, None] - per_attention_head[:, :, None, :]
    causal = (
        jnp.arange(block_rows, dtype=jnp.int32)[:, None]
        >= jnp.arange(block_rows, dtype=jnp.int32)[None, :]
    )
    decays = jnp.where(causal, jnp.exp(jnp.minimum(differences, 0.0)), 0.0)
    scaled_queries = (query_blocks * from_start[..., None]).astype(jnp.bfloat16)
    outer_terms = jnp.einsum(
        "nthd,nthe->nhde", scaled_queries, grad_blocks, preferred_element_type=jnp.float32
    )
    end_factor = jnp.exp(block_ends)
    local_total = jnp.zeros((heads_local, head_dim, head_dim), jnp.float32)
    for block_id in reversed(range(blocks)):
        local_total = end_factor[block_id][:, None, None] * local_total + outer_terms[block_id]
    all_totals, all_logs = exchange(local_total, jnp.sum(block_ends, axis=0))
    peers, place = lax.axis_size("sp"), lax.axis_index("sp")
    where = jnp.arange(peers, dtype=jnp.int32)
    between = ((where[None, :] > place) & (where[None, :] < where[:, None]))[..., None]
    reach = jnp.sum(jnp.where(between, all_logs[None], 0.0), axis=1)
    reach = jnp.where((where > place)[:, None], jnp.exp(reach), 0.0)
    suffix = jnp.sum(reach[:, :, None, None] * all_totals.astype(jnp.float32), axis=0)
    grad_dot = jnp.einsum(
        "nthe,nshe->nhts", grad_blocks, value_blocks, preferred_element_type=jnp.float32
    )
    weighted_grad = (grad_dot * decays).astype(jnp.bfloat16)
    score_dot = jnp.einsum(
        "nthd,nshd->nhts", query_blocks, key_blocks, preferred_element_type=jnp.float32
    )
    weighted_score = (score_dot * decays).astype(jnp.bfloat16)
    query_intra = jnp.einsum(
        "nhts,nshd->nthd", weighted_grad, key_blocks, preferred_element_type=jnp.float32
    )
    query_carry = jnp.einsum(
        "nthe,nhde->nthd", grad_blocks, block_states, preferred_element_type=jnp.float32
    )
    grad_queries = (
        (query_intra + query_carry * from_start[..., None])
        .astype(jnp.bfloat16)
        .reshape(tok_dev, -1)
    )
    key_intra = jnp.einsum(
        "nhts,nthd->nshd", weighted_grad, query_blocks, preferred_element_type=jnp.float32
    )
    value_intra = jnp.einsum(
        "nhts,nthe->nshe", weighted_score, grad_blocks, preferred_element_type=jnp.float32
    )
    state_grad = suffix
    leaving = []
    for block_id in reversed(range(blocks)):
        leaving.append(state_grad)
        state_grad = end_factor[block_id][:, None, None] * state_grad + outer_terms[block_id]
    carried = jnp.stack(leaving[::-1], axis=0).astype(jnp.bfloat16)
    key_carry = jnp.einsum(
        "nshe,nhde->nshd", value_blocks, carried, preferred_element_type=jnp.float32
    )
    value_carry = jnp.einsum(
        "nshd,nhde->nshe", key_blocks, carried, preferred_element_type=jnp.float32
    )
    grad_keys = (
        (key_intra + key_carry * to_end[..., None]).astype(jnp.bfloat16).reshape(tok_dev, -1)
    )
    grad_values = (
        (value_intra + value_carry * to_end[..., None]).astype(jnp.bfloat16).reshape(tok_dev, -1)
    )
    return (grad_queries, grad_keys, grad_values)


def shards(
    moe_input,
    cotangent,
    routes,
    route_weights,
    gate_weight,
    up_weight,
    down_weight,
    out_weight,
    mixer_output,
    queries,
    key_vectors,
    value_vectors,
    log_decay,
    block_states,
):
    tok_dev, model_width = cotangent.shape
    peers, parts = lax.axis_size("sp"), lax.axis_size("tp")
    capacity = 5 * tok_dev * TOP_K // (4 * peers)
    slots = pair_slots(routes, peers, capacity).reshape(tok_dev, TOP_K)
    share_width = model_width // parts
    offset = lax.axis_index("tp") * share_width
    my_inputs = lax.dynamic_slice_in_dim(moe_input, offset, share_width, 1)
    my_cotangent = lax.dynamic_slice_in_dim(cotangent, offset, share_width, 1)
    places = jnp.arange(peers * capacity, dtype=jnp.int32)
    hits = [slots[:, j][None, :] == places[:, None] for j in range(TOP_K)]
    pick = functools.reduce(jnp.logical_or, hits).astype(jnp.bfloat16)
    slot_weight = sum(
        jnp.sum(jnp.where(hits[j], route_weights[:, j][None, :], 0.0), axis=1)
        for j in range(TOP_K)
    )
    rows = (peers, capacity, share_width)
    send_inputs = jnp.dot(pick, my_inputs, preferred_element_type=jnp.float32).astype(
        jnp.bfloat16
    )
    send_grads = (
        jnp.dot(pick, my_cotangent, preferred_element_type=jnp.float32) * slot_weight[:, None]
    ).astype(jnp.bfloat16)
    arrived_inputs, arrived_grads = dispatch(
        send_inputs.reshape(rows), send_grads.reshape(rows), parts
    )
    arrived_inputs, arrived_grads, mixer_output = lax.optimization_barrier(
        (arrived_inputs, arrived_grads, mixer_output)
    )
    all_mixer = lax.all_gather(mixer_output, "sp", axis=0, tiled=True)
    input_part, grad_gate, grad_up, grad_down = expert_terms(
        arrived_inputs.reshape(peers * capacity, model_width),
        arrived_grads.reshape(peers * capacity, model_width),
        gate_weight[0],
        up_weight[0],
        down_weight[0],
    )
    place_blocks = places.reshape(peers, 1, capacity)
    combine = functools.reduce(
        jnp.logical_or, [slots[:, j][None, :, None] == place_blocks for j in range(TOP_K)]
    ).astype(jnp.bfloat16)
    residual_grad = return_rows(
        input_part.astype(jnp.bfloat16).reshape(peers, capacity, model_width),
        combine,
        my_cotangent,
    )
    grad_mix = jnp.dot(residual_grad, out_weight, preferred_element_type=jnp.float32).astype(
        jnp.bfloat16
    )
    slices = jnp.transpose(residual_grad.reshape(tok_dev, peers, model_width // peers), (1, 0, 2))
    gathered = []

    def exchange(total, logs):
        heads, head_dim, _ = total.shape
        packed = total.astype(jnp.bfloat16).reshape(-1, 128)
        wide = jnp.broadcast_to(logs[:, None], (heads, 128))
        all_res, all_tot, all_log = final_exchange(slices, packed, wide, parts)
        gathered.append(all_res)
        return all_tot.reshape((peers,) + total.shape), all_log[:, :, 0]

    grad_queries, grad_keys, grad_values = retention_grads(
        queries, key_vectors, value_vectors, grad_mix, log_decay, block_states, exchange
    )
    all_res = gathered[0].reshape(peers * tok_dev, model_width // peers)
    grad_out = contract_rows(all_res, all_mixer)
    return (
        grad_gate[None],
        grad_up[None],
        grad_down[None],
        grad_out,
        grad_queries,
        grad_keys,
        grad_values,
    )


def solution(mesh):
    return jax.shard_map(
        shards,
        mesh=mesh,
        in_specs=(
            P("sp", None),
            P("sp", None),
            P("sp", None),
            P("sp", None),
            P("sp", None, "tp"),
            P("sp", None, "tp"),
            P("sp", "tp", None),
            P(None, "tp"),
            P("sp", "tp"),
            P("sp", "tp"),
            P("sp", "tp"),
            P("sp", "tp"),
            P("sp", "tp"),
            P("sp", "tp", None, None),
        ),
        out_specs=(
            P("sp", None, "tp"),
            P("sp", None, "tp"),
            P("sp", "tp", None),
            P("sp", "tp"),
            P("sp", "tp"),
            P("sp", "tp"),
            P("sp", "tp"),
        ),
        check_vma=False,
    )
```

time: 368 us -> 235 us (0.64); the launches traced: 361 us -> 234 us
  blocking collectives: 123 us -> 0 us
  Pallas kernels: 0 us -> 121 us
  waiting for transfers between devices: 100 us -> 0.02 us
  local copies, waits for them, and re-layouts: 58.3 us -> 43.8 us
  other arithmetic: 22.3 us -> 10 us
  matrix products: 40.6 us -> 44.4 us
    pallas_call x0 -> x3, Pallas kernels: none -> 121 us  [the longest x1 46.9 us: return_rows(): pl.pallas_call(functools.partial(return_kernel, peers), out_shape=jax.Sha...]
    reduce_scatter x2 -> x0, waiting for transfers between devices: 83.9 us -> none  [the longest x1 49.4 us: shards(): lax.psum_scatter(contract_rows(residual_grad, mixer_output).astype(jnp.bf...]
    all_to_all x3 -> x0, blocking collectives: 68.7 us -> none  [the longest x1 24.9 us: shards(): lax.all_to_all(part_inputs, 'sp', split_axis=0, concat_axis=0, tiled=True)]
    all_gather x1 -> x0, blocking collectives: 35.2 us -> none  [prefix(): lax.all_gather(part.astype(kind), axis)]
    gather x3 -> x0, local copies, waits for them, and re-layouts: 19.3 us -> none  [the longest x1 8.79 us: shards(): outgoing_gradients = jnp.concatenate([scaled, zero_row], axis=0)[slot_pair]]
    unnamed x1 -> x0, blocking collectives: 19.3 us -> none
    all_gather x3 -> x1, waiting for transfers between devices: 16.2 us -> 0.01 us  [shards(): all_mixer = lax.all_gather(mixer_output, 'sp', axis=0, tiled=True)]
    select_n x10 -> x1, other arithmetic: 8.23 us -> 0.07 us  [retention_grads(): reach = jnp.where((where > place)[:, None], jnp.exp(reach), 0.0)]
  transfers between devices with their start and end apart: 5 -> 1, of which waited for: 3 -> 0; matrix products, arithmetic and copies ran while one was open for 18% -> 35% of each run, Pallas kernels for 0% -> 35%
where the time goes in v1:
time: 235 us; the launch traced here: 234 us
  Pallas kernels  121 us (51%)
  matrix products  44.4 us (19%)
  local copies, waits for them, and re-layouts  43.8 us (19%)
  between operations  14.4 us (6%)
  other arithmetic  10 us (4%)
    pallas_call x1, Pallas kernels, return_rows(): pl.pallas_call(functools.partial(return_kernel, peers), out_shape=jax.Sha...  46.9 us
    pallas_call x1, Pallas kernels, dispatch(): pl.pallas_call(functools.partial(dispatch_kernel, peers), out_shape=(out,...  39.8 us
    pallas_call x1, Pallas kernels, final_exchange(): pl.pallas_call(functools.partial(final_kernel, peers, parts), out_shape=(...  34.6 us
    dot_general x4, matrix products, contract_rows(): lax.dot_general(left, right, (((0,), (0,)), ((), ())), preferred_element_...  16.7 us
    unnamed x57, local copies, waits for them, and re-layouts  10.4 us
    mul x5, local copies, waits for them, and re-layouts, retention_grads(): end_factor[block_id][:, None, None] * local_total + outer_terms[block_id]  6.2 us
    dot_general x3, matrix products, contract_cols(): lax.dot_general(left, right, (((1,), (1,)), ((), ())), preferred_element_...  5.41 us
  transfers between devices with their start and end apart: 1, of which 0 were waited for; matrix products, arithmetic and copies ran while one was open for 35% of the time, Pallas kernels for 35%

profile of v1, /device:TPU:0, one launch (start us, length us, event | category | flops | bytes accessed | tf_op | source)
XLA Modules:
  0.0 234.0 jit_solution(6865626994315493233)
XLA Ops:
  12.7 2.1 convolution_convert_fusion
  16.3 39.8 %dispatch.1 = (bf16[8,80,2048]{2,1,0:T(8,128)(2,1)}, bf16[8,80,2048]{2,1,0:T(8,128)(2,1)}) custom-call(bf16[8,80,512]{2,1,0:T(8,128)(2,1)} %bitcast.125, bf16[8,80,512]{2,1,0:T(8,128)(2,1)} %bitcast.126), custom_call_target="tpu_custom_call" | custom-call | tf_op jit(solution)/shard_map/dispatch/pallas_call | solution.py:136
  58.4 4.0 %fusion.1 = f32[640,512]{1,0:T(8,128)S(1)} fusion(bf16[640,2048]{1,0:T(8,128)(2,1)} %bitcast.142, bf16[1,2048,512]{2,1,0:T(8,128)(2,1)} %param.19), kind=kOutput, calls=%fused_computation.5 | convolution fusion | flops 1342177280 | bytes 6029312 | tf_op jit(solution)/shard_map/dot_general | solution.py:317
  65.9 2.3 select_convert_fusion
  71.9 46.9 %return_rows.1 = bf16[256,2048]{1,0:T(8,128)(2,1)S(1)} custom-call(bf16[8,80,2048]{2,1,0:T(8,128)(2,1)S(1)} %bitcast.121, bf16[8,256,80]{2,1,0:T(8,128)(2,1)S(1)} %or_convert_fusion.pick_ref, bf16[256,512]{1,0:T(8,128)(2,1)S(1)} %constant_dynamic-slice_fusion.cot_ref), custom_call_target="tpu_custom_call" | custom-call | tf_op jit(solution)/shard_map/return_rows/pallas_call | solution.py:229
  120.1 2.3 convolution_convert_fusion.1
  129.2 1.7 squeeze.23
  130.9 1.7 squeeze.24
  133.4 1.7 mul.152
  136.5 1.7 mul.156
  139.5 1.7 add_convert_fusion.2.tot_ref
  141.9 34.6 %final_exchange.1 = (bf16[8,256,256]{2,1,0:T(8,128)(2,1)}, bf16[8,256,128]{2,1,0:T(8,128)(2,1)}, f32[8,8,128]{2,1,0:T(8,128)}) custom-call(bf16[8,256,256]{2,1,0:T(8,128)(2,1)} %bitcast.123, bf16[256,128]{1,0:T(8,128)(2,1)} %add_convert_fusion.2.tot_ref, f32[8,128]{1,0:T(8,128)} %broadcast_in_dim.113.log_ref), custom_call_target="tpu_custom_call" | custom-call | tf_op jit(solution)/shard_map/final_exchange/pallas_call | solution.py:287
  179.1 1.8 mul.164
  180.9 1.8 multiply_reduce_fusion
  182.7 1.8 reduce_sum.65
  185.1 2.1 reshape.224
  190.1 1.7 add_convert_fusion.1
  191.8 2.3 convolution_bitcast_fusion.6
  194.1 2.0 fusion.19
  200.7 1.6 fusion.10
  210.4 5.7 %convolution_bitcast_fusion.1 = f32[1,2048,512]{2,1,0:T(8,128)} fusion(bf16[640,2048]{1,0:T(8,128)(2,1)} %bitcast.143, bf16[640,512]{1,0:T(8,128)(2,1)S(1)} %copy-done.13), kind=kOutput, calls=%fused_computation.2 | convolution fusion | flops 1342177280 | bytes 7471104 | tf_op jit(solution)/shard_map/dot_general | solution.py:20
  216.1 3.9 %convolution_bitcast_fusion.2 = f32[1,2048,512]{2,1,0:T(8,128)} fusion(bf16[640,2048]{1,0:T(8,128)(2,1)S(1)} %bitcast.145, bf16[640,512]{1,0:T(8,128)(2,1)S(1)} %copy-done.11), kind=kOutput, calls=%fused_computation.3 | convolution fusion | flops 1342177280 | bytes 7471104 | tf_op jit(solution)/shard_map/dot_general | solution.py:20
  220.0 4.0 %convolution_bitcast_fusion = f32[1,512,2048]{2,1,0:T(8,128)} fusion(bf16[640,2048]{1,0:T(8,128)(2,1)S(1)} %bitcast.141, f32[640,512]{1,0:T(8,128)S(1)} %copy-done.24, f32[640,512]{1,0:T(8,128)S(1)} %copy-done.22), kind=kOutput, calls=%fused_computation.1 | convolution fusion | flops 1345454080 | bytes 9437184 | tf_op jit(solution)/shard_map/dot_general | solution.py:20
  224.0 3.1 %fusion.54 = f32[256,512]{1,0:T(8,128)} fusion(bf16[2048,256]{1,0:T(8,128)(2,1)S(1)} %bitcast.146, bf16[2048,512]{1,0:T(8,128)(2,1)} %all-gather.2.cloned.1.call-done), kind=kOutput, calls=%fused_computation.102 | convolution fusion | flops 536870912 | bytes 3670016 | tf_op jit(solution)/shard_map/dot_general | solution.py:20
  (117 shorter events, 47.2 us)
Async XLA Ops:
  7.2 55.2 %copy-start = (bf16[1,2048,512]{2,1,0:T(8,128)(2,1)S(1)}, bf16[1,2048,512]{2,1,0:T(8,128)(2,1)}, u32[]{:S(2)}) copy-start(bf16[1,2048,512]{2,1,0:T(8,128)(2,1)} %param.18) | copy-start | bytes 6291460
  7.2 216.8 %all-gather.2.cloned.1.call-start = ((), (), s32[]{:S(2)}) async-start(), calls=%async_computation | async-start | bytes 2359296 | tf_op jit(solution)/shard_map/all_gather | solution.py:468
  12.7 43.5 %copy-start.14 = (f32[256,8]{0,1:T(8,128)S(1)}, f32[256,8]{0,1:T(8,128)}, u32[]{:S(2)}) copy-start(f32[256,8]{0,1:T(8,128)} %param.26) | copy-start | bytes 24580
  58.4 4.1 %copy-start.17 = (bf16[8,80,2048]{2,1,0:T(8,128)(2,1)S(1)}, bf16[8,80,2048]{2,1,0:T(8,128)(2,1)}, u32[]{:S(2)}) copy-start(bf16[8,80,2048]{2,1,0:T(8,128)(2,1)} %get-tuple-element.17) | copy-start | bytes 7864324
  62.4 1.6 copy-start.21
  62.4 2.3 copy-start.15
  62.5 3.4 %copy-start.19 = (bf16[1,512,2048]{2,1,0:T(8,128)(2,1)S(1)}, bf16[1,512,2048]{2,1,0:T(8,128)(2,1)}, u32[]{:S(2)}) copy-start(bf16[1,512,2048]{2,1,0:T(8,128)(2,1)} %param.20) | copy-start | bytes 6291460
  64.0 4.2 %copy-start.23 = (f32[640,512]{1,0:T(8,128)}, f32[640,512]{1,0:T(8,128)S(1)}, u32[]{:S(2)}) copy-start(f32[640,512]{1,0:T(8,128)S(1)} %fusion.7) | copy-start | bytes 3932164
  68.2 1.6 copy-start.10
  68.2 1.8 copy-start.12
  68.2 2.1 copy-start.6
  126.3 12.0 %copy-start.1 = (bf16[256,2048]{0,1:T(8,128)(2,1)S(1)}, bf16[256,2048]{0,1:T(8,128)(2,1)}, u32[]{:S(2)}) copy-start(bf16[256,2048]{0,1:T(8,128)(2,1)} %copy.138) | copy-start | bytes 3145732
  182.7 7.5 %copy-start.3 = (f32[2,8,64,64]{3,2,1,0:T(8,128)S(1)}, f32[2,8,64,64]{3,2,1,0:T(8,128)}, u32[]{:S(2)}) copy-start(f32[2,8,64,64]{3,2,1,0:T(8,128)} %copy-done.2) | copy-start | bytes 786436
  182.7 9.2 %copy-start.4 = (bf16[2,128,8,64]{1,3,2,0:T(8,128)(2,1)S(1)}, bf16[2,128,8,64]{1,3,2,0:T(8,128)(2,1)}, u32[]{:S(2)}) copy-start(bf16[2,128,8,64]{1,3,2,0:T(8,128)(2,1)} %copy.142) | copy-start | bytes 786436
  191.8 2.3 copy-start.7
  200.7 2.4 %copy-start.8 = (bf16[1,8,64,64]{3,2,1,0:T(8,128)(2,1)S(1)}, bf16[1,8,64,64]{3,2,1,0:T(8,128)(2,1)}, u32[]{:S(2)}) copy-start(bf16[1,8,64,64]{3,2,1,0:T(8,128)(2,1)} %get-tuple-element.56) | copy-start | bytes 196612
  200.7 2.4 %copy-start.9 = (bf16[2,128,8,64]{1,3,2,0:T(8,128)(2,1)S(1)}, bf16[2,128,8,64]{1,3,2,0:T(8,128)(2,1)}, u32[]{:S(2)}) copy-start(bf16[2,128,8,64]{1,3,2,0:T(8,128)(2,1)} %copy.148) | copy-start | bytes 786436
  206.3 4.1 %copy-start.13 = (bf16[640,512]{1,0:T(8,128)(2,1)S(1)}, bf16[640,512]{1,0:T(8,128)(2,1)}, u32[]{:S(2)}) copy-start(bf16[640,512]{1,0:T(8,128)(2,1)} %copy-done.12) | copy-start | bytes 1966084
  210.3 5.7 %copy-start.11 = (bf16[640,512]{1,0:T(8,128)(2,1)S(1)}, bf16[640,512]{1,0:T(8,128)(2,1)}, u32[]{:S(2)}) copy-start(bf16[640,512]{1,0:T(8,128)(2,1)} %copy-done.10) | copy-start | bytes 1966084
  210.4 5.7 %copy-start.18 = (bf16[8,80,2048]{2,1,0:T(8,128)(2,1)S(1)}, bf16[8,80,2048]{2,1,0:T(8,128)(2,1)}, u32[]{:S(2)}) copy-start(bf16[8,80,2048]{2,1,0:T(8,128)(2,1)} %get-tuple-element.17) | copy-start | bytes 7864324
  216.1 3.9 %copy-start.16 = (bf16[8,80,2048]{2,1,0:T(8,128)(2,1)S(1)}, bf16[8,80,2048]{2,1,0:T(8,128)(2,1)}, u32[]{:S(2)}) copy-start(bf16[8,80,2048]{2,1,0:T(8,128)(2,1)} %get-tuple-element.18) | copy-start | bytes 7864324
  216.1 3.9 %copy-start.22 = (f32[640,512]{1,0:T(8,128)S(1)}, f32[640,512]{1,0:T(8,128)}, u32[]{:S(2)}) copy-start(f32[640,512]{1,0:T(8,128)} %copy-done.21) | copy-start | bytes 3932164
  216.1 3.9 %copy-start.24 = (f32[640,512]{1,0:T(8,128)S(1)}, f32[640,512]{1,0:T(8,128)}, u32[]{:S(2)}) copy-start(f32[640,512]{1,0:T(8,128)} %copy-done.23) | copy-start | bytes 3932164
  220.0 4.0 %copy-start.20 = (bf16[8,256,256]{2,1,0:T(8,128)(2,1)S(1)}, bf16[8,256,256]{2,1,0:T(8,128)(2,1)}, u32[]{:S(2)}) copy-start(bf16[8,256,256]{2,1,0:T(8,128)(2,1)} %get-tuple-element.19) | copy-start | bytes 3145732
  (2 other events, 1.6 us)
Sparse Core Ops, SparseCore 0:
  56.2 57.6 all-gather.1

commit v2 on v1

--- a/solution.py
+++ b/solution.py
@@ -365,9 +365,15 @@
         "nthd,nthe->nhde", scaled_queries, grad_blocks, preferred_element_type=jnp.float32
     )
     end_factor = jnp.exp(block_ends)
-    local_total = jnp.zeros((heads_local, head_dim, head_dim), jnp.float32)
-    for block_id in reversed(range(blocks)):
-        local_total = end_factor[block_id][:, None, None] * local_total + outer_terms[block_id]
+    ends_before = jnp.cumsum(block_ends, axis=0) - block_ends
+    device_start = jnp.exp(cumulative + ends_before[:, None, :])
+    total_queries = (query_blocks * device_start[..., None]).astype(jnp.bfloat16)
+    local_total = jnp.einsum(
+        "thd,the->hde",
+        total_queries.reshape(tok_dev, heads_local, head_dim),
+        grad_mix.reshape(tok_dev, heads_local, head_dim),
+        preferred_element_type=jnp.float32,
+    )
     all_totals, all_logs = exchange(local_total, jnp.sum(block_ends, axis=0))
     peers, place = lax.axis_size("sp"), lax.axis_index("sp")
     where = jnp.arange(peers, dtype=jnp.int32)
@@ -375,6 +381,7 @@
     reach = jnp.sum(jnp.where(between, all_logs[None], 0.0), axis=1)
     reach = jnp.where((where > place)[:, None], jnp.exp(reach), 0.0)
     suffix = jnp.sum(reach[:, :, None, None] * all_totals.astype(jnp.float32), axis=0)
+    suffix = suffix.reshape(heads_local, head_dim, head_dim)
     grad_dot = jnp.einsum(
         "nthe,nshe->nhts", grad_blocks, value_blocks, preferred_element_type=jnp.float32
     )
@@ -494,7 +501,7 @@
         wide = jnp.broadcast_to(logs[:, None], (heads, 128))
         all_res, all_tot, all_log = final_exchange(slices, packed, wide, parts)
         gathered.append(all_res)
-        return all_tot.reshape((peers,) + total.shape), all_log[:, :, 0]
+        return all_tot.reshape(peers, heads, -1, 128), all_log[:, :, 0]
 
     grad_queries, grad_keys, grad_values = retention_grads(
         queries, key_vectors, value_vectors, grad_mix, log_decay, block_states, exchange

time: 235 us -> 214 us (0.911)
  local copies, waits for them, and re-layouts: 43.8 us -> 28.3 us
  other arithmetic: 10 us -> 6.16 us
    mul x5 -> x1, local copies, waits for them, and re-layouts: 6.2 us -> 0.69 us  [retention_grads(): end_factor[block_id][:, None, None] * state_grad + outer_terms[block_id]]
    squeeze x2 -> x0, local copies, waits for them, and re-layouts: 3.41 us -> none  [retention_grads(): outer_terms[block_id]]
    mul x2, local copies, waits for them, and re-layouts: 3.33 us -> 0.15 us  [retention_grads(): reach[:, :, None, None] * all_totals.astype(jnp.float32)]
    unnamed x57 -> x62, local copies, waits for them, and re-layouts: 10.4 us -> 9.86 us
  transfers between devices with their start and end apart: 1 -> 1, of which waited for: 0 -> 0; matrix products, arithmetic and copies ran while one was open for 35% -> 31% of each run, Pallas kernels for 35% -> 37%
where the time goes in v2:
time: 214 us; the launch traced here: 213 us
  Pallas kernels  119 us (56%)
  matrix products  45 us (21%)
  local copies, waits for them, and re-layouts  28.3 us (13%)
  between operations  14.5 us (7%)
  other arithmetic  6.16 us (3%)
    pallas_call x1, Pallas kernels, return_rows(): pl.pallas_call(functools.partial(return_kernel, peers), out_shape=jax.Sha...  45.4 us
    pallas_call x1, Pallas kernels, dispatch(): pl.pallas_call(functools.partial(dispatch_kernel, peers), out_shape=(out,...  39.8 us
    pallas_call x1, Pallas kernels, final_exchange(): pl.pallas_call(functools.partial(final_kernel, peers, parts), out_shape=(...  33.9 us
    dot_general x4, matrix products, contract_rows(): lax.dot_general(left, right, (((0,), (0,)), ((), ())), preferred_element_...  16.7 us
    unnamed x62, local copies, waits for them, and re-layouts  9.86 us
    dot_general x3, matrix products, contract_cols(): lax.dot_general(left, right, (((1,), (1,)), ((), ())), preferred_element_...  5.41 us
  transfers between devices with their start and end apart: 1, of which 0 were waited for; matrix products, arithmetic and copies ran while one was open for 31% of the time, Pallas kernels for 37%

profile of v2, /device:TPU:0, one launch (start us, length us, event | category | flops | bytes accessed | tf_op | source)
XLA Modules:
  0.0 213.1 jit_solution(5487765363125289317)
XLA Ops:
  12.7 2.1 %convolution_convert_fusion = bf16[640,512]{1,0:T(8,128)(2,1)} fusion(s32[256]{0:T(256)S(1)} %bitcast.130, s32[256]{0:T(256)S(1)} %bitcast.126, bf16[256,2048]{1,0:T(8,128)(2,1)} %param.14, s32[]{:T(128)S(6)} %select_n.34), kind=kOutput, calls=%fused_computation.17 | convolution fusion | flops 168591360 | bytes 919556 | tf_op jit(solution)/shard_map/dot_general | solution.py:463
  16.3 39.8 %dispatch.1 = (bf16[8,80,2048]{2,1,0:T(8,128)(2,1)}, bf16[8,80,2048]{2,1,0:T(8,128)(2,1)}) custom-call(bf16[8,80,512]{2,1,0:T(8,128)(2,1)} %bitcast.121, bf16[8,80,512]{2,1,0:T(8,128)(2,1)} %bitcast.122), custom_call_target="tpu_custom_call" | custom-call | tf_op jit(solution)/shard_map/dispatch/pallas_call | solution.py:136
  57.0 4.0 %fusion.1 = f32[640,512]{1,0:T(8,128)S(1)} fusion(bf16[640,2048]{1,0:T(8,128)(2,1)} %bitcast.140, bf16[1,2048,512]{2,1,0:T(8,128)(2,1)} %param.19), kind=kOutput, calls=%fused_computation.5 | convolution fusion | flops 1342177280 | bytes 6029312 | tf_op jit(solution)/shard_map/dot_general | solution.py:317
  61.1 1.5 fusion.7
  64.4 2.3 %select_convert_fusion = (bf16[640,512]{1,0:T(8,128)(2,1)S(1)}, bf16[640,512]{1,0:T(8,128)(2,1)S(1)}) fusion(f32[640,512]{1,0:T(8,128)S(1)} %fusion.1, f32[640,512]{1,0:T(8,128)S(1)} %fusion.7, bf16[640,2048]{1,0:T(8,128)(2,1)S(1)} %bitcast.138, bf16[1,512,2048]{2,1,0:T(8,128)(2,1)S(1)} %copy-done.21), kind=kOutput, calls=%fused_computation.19 | convolution fusion | flops 1349386240 | bytes 8650752 | tf_op jit(solution)/shard_map/dot_general | solution.py:26
  66.8 1.6 fusion.5
  68.8 1.6 add_convert_fusion
  70.4 45.4 %return_rows.1 = bf16[256,2048]{1,0:T(8,128)(2,1)S(1)} custom-call(bf16[8,80,2048]{2,1,0:T(8,128)(2,1)S(1)} %bitcast.115, bf16[8,256,80]{2,1,0:T(8,128)(2,1)S(1)} %or_convert_fusion.pick_ref, bf16[256,512]{1,0:T(8,128)(2,1)S(1)} %constant_dynamic-slice_fusion.cot_ref), custom_call_target="tpu_custom_call" | custom-call | tf_op jit(solution)/shard_map/return_rows/pallas_call | solution.py:229
  115.8 1.3 copy.150
  117.2 3.0 %convolution_convert_fusion.1 = bf16[256,512]{1,0:T(8,128)(2,1)} fusion(bf16[256,2048]{1,0:T(8,128)(2,1)S(1)} %return_rows.1, bf16[2048,512]{1,0:T(8,128)(2,1)} %param.21), kind=kOutput, calls=%fused_computation.41 | convolution fusion | flops 537001984 | bytes 3407872 | tf_op jit(solution)/shard_map/dot_general | solution.py:492
  123.1 1.8 copy.152
  124.9 1.8 convolution_convert_fusion.2
  126.7 1.7 reshape.231.tot_ref
  129.7 1.3 broadcast_in_dim.111.log_ref
  131.0 33.9 %final_exchange.1 = (bf16[8,256,256]{2,1,0:T(8,128)(2,1)}, bf16[8,256,128]{2,1,0:T(8,128)(2,1)}, f32[8,8,128]{2,1,0:T(8,128)}) custom-call(bf16[8,256,256]{2,1,0:T(8,128)(2,1)} %bitcast.117, bf16[256,128]{1,0:T(8,128)(2,1)} %reshape.231.tot_ref, f32[8,128]{1,0:T(8,128)} %broadcast_in_dim.111.log_ref), custom_call_target="tpu_custom_call" | custom-call | tf_op jit(solution)/shard_map/final_exchange/pallas_call | solution.py:287
  166.0 1.4 multiply_reduce_fusion
  170.4 1.3 reshape.246
  175.0 2.3 %convolution_bitcast_fusion.6 = f32[2,128,8,64]{1,3,2,0:T(8,128)} fusion(bf16[2,128,8,64]{1,3,2,0:T(8,128)(2,1)S(1)} %copy.163, f32[2,8,128]{2,1,0:T(8,128)} %copy.160, pred[128,128]{1,0:T(8,128)(4,1)} %iota_compare_fusion.2, bf16[2,128,8,64]{1,0,3,2:T(2,128)(2,1)S(1)} %copy-done.6, bf16[2,128,8,64]{1,0,3,2:T(2,128)(2,1)S(1)} %reshape.233), kind=kOutput, calls=%fused_computation.29 | convolution fusion | flops 68419584 | bytes 1335296 | tf_op jit(solution)/shard_map/nhts,nthe->nshe/dot_general | solution.py:407
  177.2 1.4 fusion.19
  181.6 1.3 fusion.10
  189.5 5.7 %convolution_bitcast_fusion.1 = f32[1,2048,512]{2,1,0:T(8,128)} fusion(bf16[640,2048]{1,0:T(8,128)(2,1)} %bitcast.141, bf16[640,512]{1,0:T(8,128)(2,1)S(1)} %copy-done.12), kind=kOutput, calls=%fused_computation.2 | convolution fusion | flops 1342177280 | bytes 7471104 | tf_op jit(solution)/shard_map/dot_general | solution.py:20
  195.2 3.9 %convolution_bitcast_fusion.2 = f32[1,2048,512]{2,1,0:T(8,128)} fusion(bf16[640,2048]{1,0:T(8,128)(2,1)S(1)} %bitcast.143, bf16[640,512]{1,0:T(8,128)(2,1)S(1)} %copy-done.10), kind=kOutput, calls=%fused_computation.3 | convolution fusion | flops 1342177280 | bytes 7471104 | tf_op jit(solution)/shard_map/dot_general | solution.py:20
  199.1 4.0 %convolution_bitcast_fusion = f32[1,512,2048]{2,1,0:T(8,128)} fusion(bf16[640,2048]{1,0:T(8,128)(2,1)S(1)} %bitcast.139, f32[640,512]{1,0:T(8,128)S(1)} %copy-done.26, f32[640,512]{1,0:T(8,128)S(1)} %copy-done.24), kind=kOutput, calls=%fused_computation.1 | convolution fusion | flops 1345454080 | bytes 9437184 | tf_op jit(solution)/shard_map/dot_general | solution.py:20
  203.1 3.1 %fusion.66 = f32[256,512]{1,0:T(8,128)} fusion(bf16[2048,256]{1,0:T(8,128)(2,1)S(1)} %bitcast.144, bf16[2048,512]{1,0:T(8,128)(2,1)} %all-gather.2.cloned.1.call-done), kind=kOutput, calls=%fused_computation.113 | convolution fusion | flops 536870912 | bytes 3670016 | tf_op jit(solution)/shard_map/dot_general | solution.py:20
  (116 shorter events, 31.0 us)
Async XLA Ops:
  7.2 53.9 %copy-start = (bf16[1,2048,512]{2,1,0:T(8,128)(2,1)S(1)}, bf16[1,2048,512]{2,1,0:T(8,128)(2,1)}, u32[]{:S(2)}) copy-start(bf16[1,2048,512]{2,1,0:T(8,128)(2,1)} %param.18) | copy-start | bytes 6291460
  7.2 196.0 %all-gather.2.cloned.1.call-start = ((), (), s32[]{:S(2)}) async-start(), calls=%async_computation | async-start | bytes 2359296 | tf_op jit(solution)/shard_map/all_gather | solution.py:475
  12.7 43.5 %copy-start.16 = (f32[256,8]{0,1:T(8,128)S(1)}, f32[256,8]{0,1:T(8,128)}, u32[]{:S(2)}) copy-start(f32[256,8]{0,1:T(8,128)} %param.26) | copy-start | bytes 24580
  57.0 4.1 %copy-start.19 = (bf16[8,80,2048]{2,1,0:T(8,128)(2,1)S(1)}, bf16[8,80,2048]{2,1,0:T(8,128)(2,1)}, u32[]{:S(2)}) copy-start(bf16[8,80,2048]{2,1,0:T(8,128)(2,1)} %get-tuple-element.17) | copy-start | bytes 7864324
  61.1 2.2 %copy-start.17 = (bf16[8,80,2048]{2,1,0:T(8,128)(2,1)S(1)}, bf16[8,80,2048]{2,1,0:T(8,128)(2,1)}, u32[]{:S(2)}) copy-start(bf16[8,80,2048]{2,1,0:T(8,128)(2,1)} %get-tuple-element.18) | copy-start | bytes 7864324
  61.1 3.3 %copy-start.21 = (bf16[1,512,2048]{2,1,0:T(8,128)(2,1)S(1)}, bf16[1,512,2048]{2,1,0:T(8,128)(2,1)}, u32[]{:S(2)}) copy-start(bf16[1,512,2048]{2,1,0:T(8,128)(2,1)} %param.20) | copy-start | bytes 6291460
  62.6 4.1 %copy-start.25 = (f32[640,512]{1,0:T(8,128)}, f32[640,512]{1,0:T(8,128)S(1)}, u32[]{:S(2)}) copy-start(f32[640,512]{1,0:T(8,128)S(1)} %fusion.7) | copy-start | bytes 3932164
  66.8 1.8 copy-start.11
  66.8 2.1 copy-start.3
  120.2 8.2 %copy-start.1 = (bf16[256,2048]{0,1:T(8,128)(2,1)S(1)}, bf16[256,2048]{0,1:T(8,128)(2,1)}, u32[]{:S(2)}) copy-start(bf16[256,2048]{0,1:T(8,128)(2,1)} %copy.150) | copy-start | bytes 3145732
  129.6 39.1 %copy-start.2 = (bf16[256,512]{0,1:T(8,128)(2,1)S(1)}, bf16[256,512]{0,1:T(8,128)(2,1)}, u32[]{:S(2)}) copy-start(bf16[256,512]{0,1:T(8,128)(2,1)} %copy.152) | copy-start | bytes 786436
  129.6 40.0 %copy-start.15 = (f32[2,128,8]{2,1,0:T(8,128)S(1)}, f32[2,128,8]{2,1,0:T(8,128)}, u32[]{:S(2)}) copy-start(f32[2,128,8]{2,1,0:T(8,128)} %get-tuple-element.54) | copy-start | bytes 24580
  168.1 6.8 %copy-start.4 = (bf16[2,128,8,64]{1,0,3,2:T(2,128)(2,1)}, bf16[2,128,8,64]{1,0,3,2:T(2,128)(2,1)S(1)}, u32[]{:S(2)}) copy-start(bf16[2,128,8,64]{1,0,3,2:T(2,128)(2,1)S(1)} %reshape.233) | copy-start | bytes 786436
  170.4 4.6 %copy-start.6 = (bf16[2,128,8,64]{1,0,3,2:T(2,128)(2,1)S(1)}, bf16[2,128,8,64]{1,0,3,2:T(2,128)(2,1)}, u32[]{:S(2)}) copy-start(bf16[2,128,8,64]{1,0,3,2:T(2,128)(2,1)} %reshape.237) | copy-start | bytes 786436
  174.9 2.3 %copy-start.13 = (bf16[1,8,64,64]{3,2,1,0:T(8,128)(2,1)}, bf16[1,8,64,64]{3,2,1,0:T(8,128)(2,1)S(1)}, u32[]{:S(2)}) copy-start(bf16[1,8,64,64]{3,2,1,0:T(8,128)(2,1)S(1)} %fusion.21) | copy-start | bytes 196612
  177.2 4.3 %copy-start.5 = (bf16[2,128,8,64]{1,0,3,2:T(2,128)(2,1)S(1)}, bf16[2,128,8,64]{1,0,3,2:T(2,128)(2,1)}, u32[]{:S(2)}) copy-start(bf16[2,128,8,64]{1,0,3,2:T(2,128)(2,1)} %copy-done.4) | copy-start | bytes 786436
  181.6 1.6 copy-start.14
  186.4 3.1 %copy-start.12 = (bf16[640,512]{1,0:T(8,128)(2,1)S(1)}, bf16[640,512]{1,0:T(8,128)(2,1)}, u32[]{:S(2)}) copy-start(bf16[640,512]{1,0:T(8,128)(2,1)} %copy-done.11) | copy-start | bytes 1966084
  189.5 5.7 %copy-start.10 = (bf16[640,512]{1,0:T(8,128)(2,1)S(1)}, bf16[640,512]{1,0:T(8,128)(2,1)}, u32[]{:S(2)}) copy-start(bf16[640,512]{1,0:T(8,128)(2,1)} %copy-done.9) | copy-start | bytes 1966084
  189.5 5.7 %copy-start.20 = (bf16[8,80,2048]{2,1,0:T(8,128)(2,1)S(1)}, bf16[8,80,2048]{2,1,0:T(8,128)(2,1)}, u32[]{:S(2)}) copy-start(bf16[8,80,2048]{2,1,0:T(8,128)(2,1)} %get-tuple-element.17) | copy-start | bytes 7864324
  195.2 3.9 %copy-start.18 = (bf16[8,80,2048]{2,1,0:T(8,128)(2,1)S(1)}, bf16[8,80,2048]{2,1,0:T(8,128)(2,1)}, u32[]{:S(2)}) copy-start(bf16[8,80,2048]{2,1,0:T(8,128)(2,1)} %get-tuple-element.18) | copy-start | bytes 7864324
  195.2 3.9 %copy-start.24 = (f32[640,512]{1,0:T(8,128)S(1)}, f32[640,512]{1,0:T(8,128)}, u32[]{:S(2)}) copy-start(f32[640,512]{1,0:T(8,128)} %copy-done.23) | copy-start | bytes 3932164
  195.2 3.9 %copy-start.26 = (f32[640,512]{1,0:T(8,128)S(1)}, f32[640,512]{1,0:T(8,128)}, u32[]{:S(2)}) copy-start(f32[640,512]{1,0:T(8,128)} %copy-done.25) | copy-start | bytes 3932164
  199.1 4.0 %copy-start.22 = (bf16[8,256,256]{2,1,0:T(8,128)(2,1)S(1)}, bf16[8,256,256]{2,1,0:T(8,128)(2,1)}, u32[]{:S(2)}) copy-start(bf16[8,256,256]{2,1,0:T(8,128)(2,1)} %get-tuple-element.19) | copy-start | bytes 3145732
  (4 other events, 5.3 us)
Sparse Core Ops, SparseCore 0:
  56.2 56.3 all-gather.1
